TPU v7x, 32 devices: a whole 2x2x4 slice. The times are simulated.
32 devices in a mesh: grp: 2 (over y), fs: 4 (over z), tp: 4 (over x, core).
Axes of the slice: x: 2, y: 2, z: 4, core: 2. Of those that a mesh axis runs over, the one named last changes fastest.
Arguments:
- tokens: bfloat16 [2560, 2048], P(('grp', 'fs', 'tp')), parts along dimension 0, may hold values from -6 to 6
- mix_gain: bfloat16 [2048], replicated, may hold values from 0.099609375 to 1.8984375
- val_weight: bfloat16 [2048, 1024], P('fs', 'tp'), may hold values from -4 to 4
- gate_weight: bfloat16 [2048, 1024], P('fs', 'tp'), may hold values from -0.125 to 0.125
- conv_taps: bfloat16 [31, 1024], replicated, may hold values from -1 to 1
- chan_gain: bfloat16 [1024], replicated, may hold values from 0.099609375 to 1.8984375
- out_weight: bfloat16 [1024, 2048], P('tp', 'fs'), may hold values from -0.1875 to 0.1875
- mix_post_gain: bfloat16 [2048], replicated, may hold values from 0.099609375 to 1.8984375
- ffn_gain: bfloat16 [2048], replicated, may hold values from 0.099609375 to 1.8984375
- up_gate_weight: bfloat16 [2048, 5120], P('fs', 'tp'), may hold values from -0.125 to 0.125
- up_val_weight: bfloat16 [2048, 5120], P('fs', 'tp'), may hold values from -0.125 to 0.125
- ffn_taps: bfloat16 [2, 3, 5120], replicated, may hold values from -3.5 to 3.5
- down_weight: bfloat16 [5120, 2048], P('tp', 'fs'), may hold values from -0.078125 to 0.078125
- ffn_post_gain: bfloat16 [2048], replicated, may hold values from 0.099609375 to 1.8984375
Outputs:
- layer_out: bfloat16 [2560, 2048], P(('grp', 'fs', 'tp')), parts along dimension 0
There are 2 independent parts, one for each index of `grp`. A program takes and returns all parts, laid end to end along the dimension named above; an argument that names none is the same for every part. Nothing has to cross between parts.
All inputs are finite; a program needn't handle non-finite values.
Results may differ from a plain program's by a relative error of at most 0.019.
Values may be sent and summed in bfloat16 or wider, within the bound.
A program may use at most 64 MiB of HBM per device.

v0:
```python
import jax
import jax.numpy as jnp
from jax import lax
from jax.sharding import PartitionSpec as P

LEN = 64
norm_epsilon = 1e-06
chan_epsilon = 1e-05


def rms_scale(values, gain):
    inverse = lax.rsqrt(jnp.mean(values * values, axis=-1, keepdims=True) + norm_epsilon)
    return values * inverse * gain.astype(jnp.float32)


def depthwise(signal, tap_table):
    taps_count = tap_table.shape[0]
    channels = signal.shape[1]
    shaped = signal.astype(jnp.float32).reshape(signal.shape[0] // LEN, LEN, channels)
    padded = jnp.pad(shaped, ((0, 0), (taps_count - 1, 0), (0, 0)))
    tap_values = tap_table.astype(jnp.float32)
    result = jnp.zeros(shaped.shape, jnp.float32)
    for offset in range(taps_count):
        result = result + padded[:, offset : offset + LEN, :] * tap_values[offset]
    return result.reshape(signal.shape[0], channels)


def make_adder(left, pieces):
    first = jnp.dot(left, pieces[0], preferred_element_type=jnp.float32)
    second = jnp.dot(left, pieces[1], preferred_element_type=jnp.float32)
    return (first, second)


def make_rows_product(left, weight):
    return jnp.dot(left, weight, preferred_element_type=jnp.float32)


def shards(
    tokens,
    mix_gain,
    val_weight,
    gate_weight,
    conv_taps,
    chan_gain,
    out_weight,
    mix_post_gain,
    ffn_gain,
    up_gate_weight,
    up_val_weight,
    ffn_taps,
    down_weight,
    ffn_post_gain,
):
    member = lax.axis_index("tp")
    normed_own = rms_scale(tokens.astype(jnp.float32), mix_gain).astype(jnp.bfloat16)
    normed = lax.all_gather(normed_own, "tp", axis=0, tiled=True)
    local_ch = val_weight.shape[1]
    values, gate_sums = make_adder(
        normed,
        (
            lax.all_gather(val_weight, "fs", axis=0, tiled=True),
            lax.all_gather(gate_weight, "fs", axis=0, tiled=True),
        ),
    )
    glu_out = (values * jax.nn.sigmoid(gate_sums)).astype(jnp.bfloat16)
    own_taps = lax.dynamic_slice_in_dim(conv_taps, member * local_ch, local_ch, 1)
    conv_out = depthwise(glu_out, own_taps)
    totals, squares = lax.psum(
        (jnp.sum(conv_out, axis=1), jnp.sum(conv_out * conv_out, axis=1)), "tp"
    )
    all_channels = chan_gain.shape[0]
    chan_mean = totals[:, None] / all_channels
    chan_var = squares[:, None] / all_channels - chan_mean * chan_mean
    own_gain = lax.dynamic_slice_in_dim(chan_gain, member * local_ch, local_ch, 0).astype(
        jnp.float32
    )
    activated = jax.nn.silu((conv_out - chan_mean) * lax.rsqrt(chan_var + chan_epsilon) * own_gain)
    activated = activated.astype(jnp.bfloat16)
    out_full = lax.all_gather(out_weight, "fs", axis=1, tiled=True)
    mixed_sum = lax.psum_scatter(
        make_rows_product(activated, out_full).astype(jnp.bfloat16),
        "tp",
        scatter_dimension=0,
        tiled=True,
    ).astype(jnp.float32)
    residual = (tokens.astype(jnp.float32) + rms_scale(mixed_sum, mix_post_gain)).astype(
        jnp.bfloat16
    )
    normed_share = rms_scale(residual.astype(jnp.float32), ffn_gain).astype(jnp.bfloat16)
    normed_ffn = lax.all_gather(normed_share, "tp", axis=0, tiled=True)
    local_ff = up_gate_weight.shape[1]
    own_ffn_taps = lax.dynamic_slice_in_dim(ffn_taps, member * local_ff, local_ff, 2)
    gate_full, val_full = (
        lax.all_gather(up_gate_weight, "fs", axis=0, tiled=True),
        lax.all_gather(up_val_weight, "fs", axis=0, tiled=True),
    )
    up_gate = jnp.dot(normed_ffn, gate_full, preferred_element_type=jnp.float32).astype(
        jnp.bfloat16
    )
    up_val = jnp.dot(normed_ffn, val_full, preferred_element_type=jnp.float32).astype(jnp.bfloat16)
    gate_conv = depthwise(up_gate, own_ffn_taps[0])
    val_conv = depthwise(up_val, own_ffn_taps[1])
    hidden = (jax.nn.gelu(gate_conv, approximate=True) * val_conv).astype(jnp.bfloat16)
    down_full = lax.all_gather(down_weight, "fs", axis=1, tiled=True)
    ffn_sum = lax.psum_scatter(
        make_rows_product(hidden, down_full).astype(jnp.bfloat16),
        "tp",
        scatter_dimension=0,
        tiled=True,
    ).astype(jnp.float32)
    return (residual.astype(jnp.float32) + rms_scale(ffn_sum, ffn_post_gain)).astype(jnp.bfloat16)


def solution(mesh):
    return jax.shard_map(
        shards,
        mesh=mesh,
        in_specs=(
            P(("grp", "fs", "tp"), None),
            P(),
            P("fs", "tp"),
            P("fs", "tp"),
            P(),
            P(),
            P("tp", "fs"),
            P(),
            P(),
            P("fs", "tp"),
            P("fs", "tp"),
            P(),
            P("tp", "fs"),
            P(),
        ),
        out_specs=P(("grp", "fs", "tp"), None),
        check_vma=False,
    )
```

profile of v0, /device:TPU:0, one launch (start us, length us, event | category | flops | bytes accessed | tf_op | source)
XLA Modules:
  0.0 503.6 jit_solution(17224619364062690328)
XLA Ops:
  8.0 1.1 fusion.26
  9.1 1.8 fusion.28
  13.9 25.7 %all-gather.11.cloned.1.call-done = bf16[2048,256]{1,0:T(8,128)(2,1)} async-done(((bf16[512,256]{1,0:T(8,128)(2,1)}), bf16[2048,256]{1,0:T(8,128)(2,1)}) %all-gather.11.cloned.1.call-update) | async-done | bytes 1048592 | tf_op jit(solution)/shard_map/all_gather | solution.py:61
  39.7 19.1 %all-gather.9.cloned.1.call-done = bf16[320,2048]{1,0:T(8,128)(2,1)} async-done(((bf16[80,2048]{1,0:T(8,128)(2,1)}), bf16[320,2048]{1,0:T(8,128)(2,1)}) %all-gather.9.cloned.1.call-update) | async-done | bytes 1310736 | tf_op jit(solution)/shard_map/all_gather | solution.py:56
  58.8 2.2 fusion.101
  61.0 27.4 %all-gather.13.cloned.1.call-done = bf16[2048,256]{1,0:T(8,128)(2,1)} async-done(((bf16[512,256]{1,0:T(8,128)(2,1)}), bf16[2048,256]{1,0:T(8,128)(2,1)}) %all-gather.13.cloned.1.call-update) | async-done | bytes 1048592 | tf_op jit(solution)/shard_map/all_gather | solution.py:62
  88.4 1.7 fusion.21
  90.2 1.2 fusion.96
  91.5 6.1 %all-reduce.3 = (f32[320]{0:T(512)S(1)}, f32[320]{0:T(512)S(1)}) all-reduce(f32[320]{0:T(512)S(1)} %reduce_sum.62, f32[320]{0:T(512)S(1)} %reduce_sum.60), channel_id=1, replica_groups=mesh['grp'=2,'fs'=4,'tp'=4] {'tp'}, use_global_device_ids=true, to_apply=%region_4.5 | all-reduce | flops 640 | bytes 5120 | tf_op jit(solution)/shard_map/psum | solution.py:68
  97.8 19.4 %all-gather.15.cloned.1.call-done = bf16[256,2048]{1,0:T(8,128)(2,1)} async-done(((bf16[256,512]{1,0:T(8,128)(2,1)}), bf16[256,2048]{1,0:T(8,128)(2,1)}) %all-gather.15.cloned.1.call-update) | async-done | bytes 1048592 | tf_op jit(solution)/shard_map/all_gather | solution.py:79
  117.2 2.8 convolution_convert_fusion.3
  120.1 25.9 %reduce-scatter.3.cloned.1.call-done = bf16[80,2048]{1,0:T(8,128)(2,1)} async-done(((bf16[320,2048]{1,0:T(8,128)(2,1)}), bf16[80,2048]{1,0:T(8,128)(2,1)}) %reduce-scatter.3.cloned.1.call-update) | async-done | bytes 327696 | tf_op jit(solution)/shard_map/reduce_scatter | solution.py:80
  146.0 1.1 fusion.22
  147.1 1.3 fusion.30
  151.9 15.8 %all-gather.17.cloned.1.call-done = bf16[320,2048]{1,0:T(8,128)(2,1)} async-done(((bf16[80,2048]{1,0:T(8,128)(2,1)}), bf16[320,2048]{1,0:T(8,128)(2,1)}) %all-gather.17.cloned.1.call-update) | async-done | bytes 1310736 | tf_op jit(solution)/shard_map/all_gather | solution.py:90
  167.7 99.6 %all-gather.19.cloned.1.call-done = bf16[2048,1280]{1,0:T(8,128)(2,1)} async-done(((bf16[512,1280]{1,0:T(8,128)(2,1)}), bf16[2048,1280]{1,0:T(8,128)(2,1)}) %all-gather.19.cloned.1.call-update) | async-done | bytes 5242896 | tf_op jit(solution)/shard_map/all_gather | solution.py:94
  267.3 4.8 convolution_convert_fusion.2
  272.2 93.1 %all-gather.21.cloned.1.call-done = bf16[2048,1280]{1,0:T(8,128)(2,1)} async-done(((bf16[512,1280]{1,0:T(8,128)(2,1)}), bf16[2048,1280]{1,0:T(8,128)(2,1)}) %all-gather.21.cloned.1.call-update) | async-done | bytes 5242896 | tf_op jit(solution)/shard_map/all_gather | solution.py:95
  365.3 4.3 convolution_convert_fusion.1
  371.3 92.0 %all-gather.23.cloned.1.call-done = bf16[1280,2048]{1,0:T(8,128)(2,1)} async-done(((bf16[1280,512]{1,0:T(8,128)(2,1)}), bf16[1280,2048]{1,0:T(8,128)(2,1)}) %all-gather.23.cloned.1.call-update) | async-done | bytes 5242896 | tf_op jit(solution)/shard_map/all_gather | solution.py:104
  463.3 5.5 %convolution_convert_fusion = bf16[320,2048]{1,0:T(8,128)(2,1)} fusion(bf16[320,1280]{1,0:T(8,128)(2,1)S(1)} %fusion.16, bf16[1280,2048]{1,0:T(8,128)(2,1)} %all-gather.23.cloned.1.call-done), kind=kOutput, calls=%fused_computation | convolution fusion | flops 1678376960 | bytes 7372800 | tf_op jit(solution)/shard_map/dot_general | solution.py:35
  468.8 24.9 %reduce-scatter.5.cloned.1.call-done = bf16[80,2048]{1,0:T(8,128)(2,1)} async-done(((bf16[320,2048]{1,0:T(8,128)(2,1)}), bf16[80,2048]{1,0:T(8,128)(2,1)}) %reduce-scatter.5.cloned.1.call-update) | async-done | bytes 327696 | tf_op jit(solution)/shard_map/reduce_scatter | solution.py:105
  493.7 1.1 fusion.24
  494.9 1.9 fusion.33
  (59 shorter events, 9.9 us)
Async XLA Ops:
  6.5 33.1 %all-gather.11.cloned.1.call-start = ((), (), s32[]{:S(2)}) async-start(), calls=%async_computation.3 | async-start | bytes 1310720 | tf_op jit(solution)/shard_map/all_gather | solution.py:61
  7.3 51.5 %all-gather.9.cloned.1.call-start = ((), (), s32[]{:S(2)}) async-start(), calls=%async_computation.2 | async-start | bytes 1638400 | tf_op jit(solution)/shard_map/all_gather | solution.py:56
  11.0 77.4 %all-gather.13.cloned.1.call-start = ((), (), s32[]{:S(2)}) async-start(), calls=%async_computation.4 | async-start | bytes 1310720 | tf_op jit(solution)/shard_map/all_gather | solution.py:62
  11.8 105.4 %all-gather.15.cloned.1.call-start = ((), (), s32[]{:S(2)}) async-start(), calls=%async_computation.5 | async-start | bytes 1310720 | tf_op jit(solution)/shard_map/all_gather | solution.py:79
  12.3 133.6 %reduce-scatter.3.cloned.1.call-start = ((), (), s32[]{:S(2)}) async-start(), calls=%async_computation.6 | async-start | bytes 1638400 | tf_op jit(solution)/shard_map/reduce_scatter | solution.py:80
  58.8 29.6 %copy-start.5 = (bf16[320,2048]{1,0:T(8,128)(2,1)S(1)}, bf16[320,2048]{1,0:T(8,128)(2,1)}, u32[]{:S(2)}) copy-start(bf16[320,2048]{1,0:T(8,128)(2,1)} %all-gather.9.cloned.1.call-done) | copy-start | bytes 3932164
  97.8 22.3 %copy-start.2 = (bf16[2048]{0:T(1024)(128)(2,1)S(1)}, bf16[2048]{0:T(1024)(128)(2,1)}, u32[]{:S(2)}) copy-start(bf16[2048]{0:T(1024)(128)(2,1)} %param.21) | copy-start | bytes 12292
  97.8 22.3 %copy-start.3 = (bf16[2048]{0:T(1024)(128)(2,1)S(1)}, bf16[2048]{0:T(1024)(128)(2,1)}, u32[]{:S(2)}) copy-start(bf16[2048]{0:T(1024)(128)(2,1)} %param.22) | copy-start | bytes 12292
  97.8 49.3 %copy-start = (bf16[80,2048]{1,0:T(8,128)(2,1)S(1)}, bf16[80,2048]{1,0:T(8,128)(2,1)}, u32[]{:S(2)}) copy-start(bf16[80,2048]{1,0:T(8,128)(2,1)} %param.14) | copy-start | bytes 983044
  120.0 47.7 %all-gather.17.cloned.1.call-start = ((), (), s32[]{:S(2)}) async-start(), calls=%async_computation.7 | async-start | bytes 1638400 | tf_op jit(solution)/shard_map/all_gather | solution.py:90
  149.4 118.0 %all-gather.19.cloned.1.call-start = ((), (), s32[]{:S(2)}) async-start(), calls=%async_computation.8 | async-start | bytes 6553600 | tf_op jit(solution)/shard_map/all_gather | solution.py:94
  150.1 1.5 copy-start.1
  150.1 215.2 %all-gather.21.cloned.1.call-start = ((), (), s32[]{:S(2)}) async-start(), calls=%async_computation.9 | async-start | bytes 6553600 | tf_op jit(solution)/shard_map/all_gather | solution.py:95
  150.9 312.4 %all-gather.23.cloned.1.call-start = ((), (), s32[]{:S(2)}) async-start(), calls=%async_computation.10 | async-start | bytes 6553600 | tf_op jit(solution)/shard_map/all_gather | solution.py:104
  151.6 342.1 %reduce-scatter.5.cloned.1.call-start = ((), (), s32[]{:S(2)}) async-start(), calls=%async_computation.11 | async-start | bytes 1638400 | tf_op jit(solution)/shard_map/reduce_scatter | solution.py:105
  272.1 93.2 %copy-start.6 = (bf16[320,2048]{1,0:T(8,128)(2,1)S(1)}, bf16[320,2048]{1,0:T(8,128)(2,1)}, u32[]{:S(2)}) copy-start(bf16[320,2048]{1,0:T(8,128)(2,1)} %all-gather.17.cloned.1.call-done) | copy-start | bytes 3932164
  371.3 97.5 %copy-start.4 = (bf16[2048]{0:T(1024)(128)(2,1)S(1)}, bf16[2048]{0:T(1024)(128)(2,1)}, u32[]{:S(2)}) copy-start(bf16[2048]{0:T(1024)(128)(2,1)} %param.27) | copy-start | bytes 12292
Sparse Core Ops, SparseCore 0:
  8.9 30.7 all-gather.10
  41.2 17.5 all-gather.8
  60.4 27.9 all-gather.12
  89.8 27.3 all-gather.14
  120.1 25.7 reduce-scatter.2
  149.5 18.1 all-gather.16
  169.3 98.0 all-gather.18
  268.9 96.3 all-gather.20
  366.9 96.3 all-gather.22
  468.9 24.7 reduce-scatter.4
where the time goes:
time: 504 us
  waiting for transfers between devices  447 us (89%)
  matrix products  21.4 us (4%)
  other arithmetic  14.9 us (3%)
  between operations  13.8 us (3%)
  blocking collectives  6.05 us (1%)
    all_gather x1, waiting for transfers between devices, shards(): lax.all_gather(up_gate_weight, 'fs', axis=0, tiled=True)  99.6 us
    all_gather x1, waiting for transfers between devices, shards(): lax.all_gather(up_val_weight, 'fs', axis=0, tiled=True)  93.1 us
    all_gather x1, waiting for transfers between devices, shards(): down_full = lax.all_gather(down_weight, 'fs', axis=1, tiled=True)  92 us
    all_gather x1, waiting for transfers between devices, shards(): lax.all_gather(gate_weight, 'fs', axis=0, tiled=True)  27.4 us
    reduce_scatter x1, waiting for transfers between devices, shards(): lax.psum_scatter(make_rows_product(activated, out_full).astype(jnp.bfloat...  25.9 us
    all_gather x1, waiting for transfers between devices, shards(): lax.all_gather(val_weight, 'fs', axis=0, tiled=True)  25.7 us
    reduce_scatter x1, waiting for transfers between devices, shards(): lax.psum_scatter(make_rows_product(hidden, down_full).astype(jnp.bfloat16...  24.9 us
    all_gather x1, waiting for transfers between devices, shards(): out_full = lax.all_gather(out_weight, 'fs', axis=1, tiled=True)  19.4 us
  transfers between devices with their start and end apart: 10, of which 10 were waited for; matrix products, arithmetic and copies ran while one was open for 4% of the time, Pallas kernels for 0%

commit v1 on v0

--- a/solution.py
+++ b/solution.py
@@ -6,6 +6,12 @@
 LEN = 64
 norm_epsilon = 1e-06
 chan_epsilon = 1e-05
+
+
+def stack_and_merge(array, axis, dim):
+    blocks = lax.all_gather(array, axis, axis=0, tiled=False)
+    whole = jnp.concatenate(blocks, axis=dim)
+    return whole
 
 
 def rms_scale(values, gain):
@@ -101,7 +107,7 @@
     gate_conv = depthwise(up_gate, own_ffn_taps[0])
     val_conv = depthwise(up_val, own_ffn_taps[1])
     hidden = (jax.nn.gelu(gate_conv, approximate=True) * val_conv).astype(jnp.bfloat16)
-    down_full = lax.all_gather(down_weight, "fs", axis=1, tiled=True)
+    down_full = stack_and_merge(down_weight, "fs", 1)
     ffn_sum = lax.psum_scatter(
         make_rows_product(hidden, down_full).astype(jnp.bfloat16),
         "tp",

time: 504 us -> 514 us (1.020)
  local copies, waits for them, and re-layouts: 0.3 us -> 8.87 us
    reshape x0 -> x1, local copies, waits for them, and re-layouts: none -> 7.86 us  [stack_and_merge(): whole = jnp.concatenate(blocks, axis=dim)]
where the time goes in v1:
time: 514 us
  waiting for transfers between devices  448 us (87%)
  matrix products  21.3 us (4%)
  other arithmetic  14.8 us (3%)
  between operations  13.8 us (3%)
  local copies, waits for them, and re-layouts  8.87 us (2%)
  blocking collectives  6.05 us (1%)
    all_gather x1, waiting for transfers between devices, shards(): lax.all_gather(up_gate_weight, 'fs', axis=0, tiled=True)  99.6 us
    all_gather x1, waiting for transfers between devices, stack_and_merge(): blocks = lax.all_gather(array, axis, axis=0, tiled=False)  93.5 us
    all_gather x1, waiting for transfers between devices, shards(): lax.all_gather(up_val_weight, 'fs', axis=0, tiled=True)  93.1 us
    all_gather x1, waiting for transfers between devices, shards(): lax.all_gather(gate_weight, 'fs', axis=0, tiled=True)  27.4 us
    reduce_scatter x1, waiting for transfers between devices, shards(): lax.psum_scatter(make_rows_product(activated, out_full).astype(jnp.bfloat...  25.9 us
    all_gather x1, waiting for transfers between devices, shards(): lax.all_gather(val_weight, 'fs', axis=0, tiled=True)  25.7 us
    reduce_scatter x1, waiting for transfers between devices, shards(): lax.psum_scatter(make_rows_product(hidden, down_full).astype(jnp.bfloat16...  24.9 us
    all_gather x1, waiting for transfers between devices, shards(): out_full = lax.all_gather(out_weight, 'fs', axis=1, tiled=True)  19.4 us
  transfers between devices with their start and end apart: 10, of which 10 were waited for; matrix products, arithmetic and copies ran while one was open for 4% of the time, Pallas kernels for 0%

profile of v1, /device:TPU:0, one launch (start us, length us, event | category | flops | bytes accessed | tf_op | source)
XLA Modules:
  0.0 513.7 jit_solution(4863321637175996717)
XLA Ops:
  8.0 1.1 fusion.26
  9.1 1.8 fusion.28
  13.9 25.7 %all-gather.12.cloned.1.call-done = bf16[2048,256]{1,0:T(8,128)(2,1)} async-done(((bf16[512,256]{1,0:T(8,128)(2,1)}), bf16[2048,256]{1,0:T(8,128)(2,1)}) %all-gather.12.cloned.1.call-update) | async-done | bytes 1048592 | tf_op jit(solution)/shard_map/all_gather | solution.py:67
  39.7 19.1 %all-gather.10.cloned.1.call-done = bf16[320,2048]{1,0:T(8,128)(2,1)} async-done(((bf16[80,2048]{1,0:T(8,128)(2,1)}), bf16[320,2048]{1,0:T(8,128)(2,1)}) %all-gather.10.cloned.1.call-update) | async-done | bytes 1310736 | tf_op jit(solution)/shard_map/all_gather | solution.py:62
  58.8 2.2 fusion.101
  61.0 27.4 %all-gather.14.cloned.1.call-done = bf16[2048,256]{1,0:T(8,128)(2,1)} async-done(((bf16[512,256]{1,0:T(8,128)(2,1)}), bf16[2048,256]{1,0:T(8,128)(2,1)}) %all-gather.14.cloned.1.call-update) | async-done | bytes 1048592 | tf_op jit(solution)/shard_map/all_gather | solution.py:68
  88.4 1.8 fusion.21
  90.2 1.2 fusion.96
  91.5 6.1 %all-reduce.3 = (f32[320]{0:T(512)S(1)}, f32[320]{0:T(512)S(1)}) all-reduce(f32[320]{0:T(512)S(1)} %reduce_sum.62, f32[320]{0:T(512)S(1)} %reduce_sum.60), channel_id=1, replica_groups=mesh['grp'=2,'fs'=4,'tp'=4] {'tp'}, use_global_device_ids=true, to_apply=%region_4.5 | all-reduce | flops 640 | bytes 5120 | tf_op jit(solution)/shard_map/psum | solution.py:74
  97.8 19.4 %all-gather.16.cloned.1.call-done = bf16[256,2048]{1,0:T(8,128)(2,1)} async-done(((bf16[256,512]{1,0:T(8,128)(2,1)}), bf16[256,2048]{1,0:T(8,128)(2,1)}) %all-gather.16.cloned.1.call-update) | async-done | bytes 1048592 | tf_op jit(solution)/shard_map/all_gather | solution.py:85
  117.2 2.8 convolution_convert_fusion.3
  120.1 25.9 %reduce-scatter.3.cloned.1.call-done = bf16[80,2048]{1,0:T(8,128)(2,1)} async-done(((bf16[320,2048]{1,0:T(8,128)(2,1)}), bf16[80,2048]{1,0:T(8,128)(2,1)}) %reduce-scatter.3.cloned.1.call-update) | async-done | bytes 327696 | tf_op jit(solution)/shard_map/reduce_scatter | solution.py:86
  147.1 1.3 fusion.30
  152.6 15.8 %all-gather.18.cloned.1.call-done = bf16[320,2048]{1,0:T(8,128)(2,1)} async-done(((bf16[80,2048]{1,0:T(8,128)(2,1)}), bf16[320,2048]{1,0:T(8,128)(2,1)}) %all-gather.18.cloned.1.call-update) | async-done | bytes 1310736 | tf_op jit(solution)/shard_map/all_gather | solution.py:96
  168.4 99.6 %all-gather.20.cloned.1.call-done = bf16[2048,1280]{1,0:T(8,128)(2,1)} async-done(((bf16[512,1280]{1,0:T(8,128)(2,1)}), bf16[2048,1280]{1,0:T(8,128)(2,1)}) %all-gather.20.cloned.1.call-update) | async-done | bytes 5242896 | tf_op jit(solution)/shard_map/all_gather | solution.py:100
  268.0 4.7 convolution_convert_fusion.2
  272.9 93.1 %all-gather.22.cloned.1.call-done = bf16[2048,1280]{1,0:T(8,128)(2,1)} async-done(((bf16[512,1280]{1,0:T(8,128)(2,1)}), bf16[2048,1280]{1,0:T(8,128)(2,1)}) %all-gather.22.cloned.1.call-update) | async-done | bytes 5242896 | tf_op jit(solution)/shard_map/all_gather | solution.py:101
  366.0 4.3 convolution_convert_fusion.1
  370.5 93.5 %all-gather.24.cloned.1.call-done = bf16[5120,512]{1,0:T(8,128)(2,1)} async-done(((bf16[1280,512]{1,0:T(8,128)(2,1)}), bf16[5120,512]{1,0:T(8,128)(2,1)}) %all-gather.24.cloned.1.call-update) | async-done | bytes 5242896 | tf_op jit(solution)/shard_map/all_gather | solution.py:12
  464.0 7.9 %copy.15 = bf16[1280,4,512]{0,2,1:T(8,128)(2,1)} copy(bf16[1280,4,512]{2,0,1:T(8,128)(2,1)} %bitcast.62) | data formatting | bytes 10485760 | tf_op jit(solution)/shard_map/reshape | solution.py:13
  471.9 1.5 fusion.8
  473.4 5.4 %convolution_convert_fusion = bf16[320,2048]{1,0:T(8,128)(2,1)} fusion(bf16[320,1280]{1,0:T(8,128)(2,1)S(1)} %bitcast.66, bf16[1280,2048]{0,1:T(8,128)(2,1)} %bitcast.63), kind=kOutput, calls=%fused_computation | convolution fusion | flops 1678376960 | bytes 7372800 | tf_op jit(solution)/shard_map/dot_general | solution.py:41
  478.9 24.9 %reduce-scatter.5.cloned.1.call-done = bf16[80,2048]{1,0:T(8,128)(2,1)} async-done(((bf16[320,2048]{1,0:T(8,128)(2,1)}), bf16[80,2048]{1,0:T(8,128)(2,1)}) %reduce-scatter.5.cloned.1.call-update) | async-done | bytes 327696 | tf_op jit(solution)/shard_map/reduce_scatter | solution.py:111
  504.9 1.9 fusion.33
  (62 shorter events, 11.4 us)
Async XLA Ops:
  6.5 33.1 %all-gather.12.cloned.1.call-start = ((), (), s32[]{:S(2)}) async-start(), calls=%async_computation.3 | async-start | bytes 1310720 | tf_op jit(solution)/shard_map/all_gather | solution.py:67
  7.3 51.5 %all-gather.10.cloned.1.call-start = ((), (), s32[]{:S(2)}) async-start(), calls=%async_computation.2 | async-start | bytes 1638400 | tf_op jit(solution)/shard_map/all_gather | solution.py:62
  11.0 77.4 %all-gather.14.cloned.1.call-start = ((), (), s32[]{:S(2)}) async-start(), calls=%async_computation.4 | async-start | bytes 1310720 | tf_op jit(solution)/shard_map/all_gather | solution.py:68
  11.8 105.4 %all-gather.16.cloned.1.call-start = ((), (), s32[]{:S(2)}) async-start(), calls=%async_computation.5 | async-start | bytes 1310720 | tf_op jit(solution)/shard_map/all_gather | solution.py:85
  12.3 133.6 %reduce-scatter.3.cloned.1.call-start = ((), (), s32[]{:S(2)}) async-start(), calls=%async_computation.6 | async-start | bytes 1638400 | tf_op jit(solution)/shard_map/reduce_scatter | solution.py:86
  58.8 29.6 %copy-start.7 = (bf16[320,2048]{1,0:T(8,128)(2,1)S(1)}, bf16[320,2048]{1,0:T(8,128)(2,1)}, u32[]{:S(2)}) copy-start(bf16[320,2048]{1,0:T(8,128)(2,1)} %all-gather.10.cloned.1.call-done) | copy-start | bytes 3932164
  97.8 22.3 %copy-start.4 = (bf16[2048]{0:T(1024)(128)(2,1)S(1)}, bf16[2048]{0:T(1024)(128)(2,1)}, u32[]{:S(2)}) copy-start(bf16[2048]{0:T(1024)(128)(2,1)} %param.21) | copy-start | bytes 12292
  97.8 22.3 %copy-start.5 = (bf16[2048]{0:T(1024)(128)(2,1)S(1)}, bf16[2048]{0:T(1024)(128)(2,1)}, u32[]{:S(2)}) copy-start(bf16[2048]{0:T(1024)(128)(2,1)} %param.22) | copy-start | bytes 12292
  97.8 49.3 %copy-start.2 = (bf16[80,2048]{1,0:T(8,128)(2,1)S(1)}, bf16[80,2048]{1,0:T(8,128)(2,1)}, u32[]{:S(2)}) copy-start(bf16[80,2048]{1,0:T(8,128)(2,1)} %param.14) | copy-start | bytes 983044
  120.0 48.4 %all-gather.18.cloned.1.call-start = ((), (), s32[]{:S(2)}) async-start(), calls=%async_computation.7 | async-start | bytes 1638400 | tf_op jit(solution)/shard_map/all_gather | solution.py:96
  148.5 0.7 copy-start
  150.1 118.0 %all-gather.20.cloned.1.call-start = ((), (), s32[]{:S(2)}) async-start(), calls=%async_computation.8 | async-start | bytes 6553600 | tf_op jit(solution)/shard_map/all_gather | solution.py:100
  150.8 1.5 copy-start.3
  150.8 215.2 %all-gather.22.cloned.1.call-start = ((), (), s32[]{:S(2)}) async-start(), calls=%async_computation.9 | async-start | bytes 6553600 | tf_op jit(solution)/shard_map/all_gather | solution.py:101
  151.6 312.4 %all-gather.24.cloned.1.call-start = ((), (), s32[]{:S(2)}) async-start(), calls=%async_computation.11 | async-start | bytes 6553600 | tf_op jit(solution)/shard_map/all_gather | solution.py:12
  152.3 351.5 %reduce-scatter.5.cloned.1.call-start = ((), (), s32[]{:S(2)}) async-start(), calls=%async_computation.10 | async-start | bytes 1638400 | tf_op jit(solution)/shard_map/reduce_scatter | solution.py:111
  272.8 93.2 %copy-start.8 = (bf16[320,2048]{1,0:T(8,128)(2,1)S(1)}, bf16[320,2048]{1,0:T(8,128)(2,1)}, u32[]{:S(2)}) copy-start(bf16[320,2048]{1,0:T(8,128)(2,1)} %all-gather.18.cloned.1.call-done) | copy-start | bytes 3932164
  473.4 5.5 %copy-start.6 = (bf16[2048]{0:T(1024)(128)(2,1)S(1)}, bf16[2048]{0:T(1024)(128)(2,1)}, u32[]{:S(2)}) copy-start(bf16[2048]{0:T(1024)(128)(2,1)} %param.27) | copy-start | bytes 12292
  478.8 26.1 %copy-start.1 = (bf16[80,2048]{1,0:T(8,128)(2,1)S(1)}, bf16[80,2048]{1,0:T(8,128)(2,1)}, u32[]{:S(2)}) copy-start(bf16[80,2048]{1,0:T(8,128)(2,1)} %copy-done) | copy-start | bytes 983044
Sparse Core Ops, SparseCore 0:
  8.9 30.7 all-gather.11
  41.2 17.5 all-gather.9
  60.4 27.9 all-gather.13
  89.8 27.3 all-gather.15
  120.1 25.7 reduce-scatter.2
  150.2 18.1 all-gather.17
  170.0 98.0 all-gather.19
  269.6 96.3 all-gather.21
  367.6 96.3 all-gather.23
  479.0 24.7 reduce-scatter.4
